TPU v7x, 32 devices: a whole 2x2x4 slice. The times are simulated.
32 devices in a mesh: sp: 8 (over z, y), tp: 4 (over x, core).
Axes of the slice: x: 2, y: 2, z: 4, core: 2. Of those that a mesh axis runs over, the one named last changes fastest.
Arguments:
- queries: bfloat16 [6144, 2048], P('sp', 'tp'), may hold values from -11 to 11
- key_rows: bfloat16 [6144, 2048], P('sp', 'tp'), may hold values from -4.5 to 4.5
- value_rows: bfloat16 [6144, 2048], P('sp', 'tp'), may hold values from -6 to 6
- log_forget: float32 [6144, 32], P('sp', 'tp'), may hold values from -740.28 to 0, as said below
- stream_in: bfloat16 [6144, 2048], P('sp'), may hold values from -6 to 6
- out_weight: bfloat16 [2048, 2048], P('tp'), may hold values from -0.52734375 to 0.52734375
- mix_gain: float32 [2048], replicated, may hold values from 0.1 to 1.9
- mix_bias: float32 [2048], replicated, may hold values from -3 to 3
- gate_weight: bfloat16 [2048, 5632], P('sp', 'tp'), may hold values from -0.125 to 0.125
- up_weight: bfloat16 [2048, 5632], P('sp', 'tp'), may hold values from -0.125 to 0.125
- down_weight: bfloat16 [5632, 2048], P('tp', 'sp'), may hold values from -0.15917969 to 0.15917969
- ffn_gain: float32 [2048], replicated, may hold values from 0.1 to 1.9
- ffn_bias: float32 [2048], replicated, may hold values from -3 to 3
Outputs:
- layer_out: bfloat16 [6144, 2048], P(('sp', 'tp'))
Inputs may be any that keep to these rules, and one draw needn't show every extreme that they name: `log_forget`: each column never rises along the positions.
All inputs are finite; a program needn't handle non-finite values.
Results may differ from a plain program's by a relative error of at most 0.015.
Values may be sent and summed in bfloat16 or wider, within the bound.
A program may use at most 128 MiB of HBM per device.

v0:
```python
import jax
import jax.numpy as jnp
from jax import lax
from jax.sharding import PartitionSpec as P

ALPHA = 8.0**0.25
EPSILON = 1e-05


def layer_norm(matrix, norm_gain, norm_shift):
    centred = matrix - jnp.mean(matrix, axis=-1, keepdims=True)
    spread = jnp.mean(centred * centred, axis=-1, keepdims=True)
    return centred * lax.rsqrt(spread + EPSILON) * norm_gain + norm_shift


def attend(queries, key_rows, value_rows, log_forget):
    length, row_width = queries.shape
    head_count = log_forget.shape[1]
    head_dim = row_width // head_count
    score_scale = head_dim ** (-0.5)
    first_pos = lax.axis_index("sp") * length
    last_pos = first_pos + length
    query_heads = queries.reshape(length, head_count, head_dim)
    query_gates = log_forget.T
    query_pos = first_pos + jnp.arange(length, dtype=jnp.int32)
    gates_all = lax.all_gather(log_forget, "sp", axis=0, tiled=True)
    initial = (
        jnp.full((head_count, length), -1e30, jnp.float32),
        jnp.zeros((head_count, length), jnp.float32),
        jnp.zeros((length, head_count, head_dim), jnp.float32),
    )
    running = initial
    key_piece = lax.all_gather(key_rows, "sp", axis=0, tiled=True)
    value_piece = lax.all_gather(value_rows, "sp", axis=0, tiled=True)
    piece_len = key_piece.shape[0]
    shards = piece_len // length
    group_size = max(
        [
            count_try
            for count_try in range(1, shards + 1)
            if shards % count_try == 0 and count_try * length <= max(length, 512)
        ]
    )
    block_len = group_size * length
    blocks = piece_len // block_len
    key_blocks = key_piece.reshape(blocks, block_len, head_count, head_dim)
    value_blocks = value_piece.reshape(blocks, block_len, head_count, head_dim)
    gate_blocks = gates_all.reshape(blocks, block_len, head_count)
    block_starts = block_len * jnp.arange(blocks, dtype=jnp.int32)

    def one_block(running_state, packed):
        key_block, value_block, gate_block, block_start = packed

        def compute(state_in):
            highest, totals, weighted = state_in
            scores = (
                jnp.einsum(
                    "qhd,khd->hqk", query_heads, key_block, preferred_element_type=jnp.float32
                )
                * score_scale
            )
            scores = scores + query_gates[:, :, None] - gate_block.T[:, None, :]
            key_pos = block_start + jnp.arange(block_len, dtype=jnp.int32)
            allowed = (key_pos[None, :] <= query_pos[:, None])[None]
            masked = jnp.where(allowed, scores, -1e30)
            new_high = jnp.maximum(highest, jnp.max(masked, axis=2))
            weights = jnp.where(allowed, jnp.exp(masked - new_high[:, :, None]), 0.0)
            factor = jnp.exp(highest - new_high)
            totals = totals * factor + jnp.sum(weights, axis=2)
            weighted = weighted * factor.T[:, :, None] + jnp.einsum(
                "hqk,khd->qhd",
                weights.astype(jnp.bfloat16),
                value_block,
                preferred_element_type=jnp.float32,
            )
            return (new_high, totals, weighted)

        def keep_state(state_in):
            return state_in

        return (lax.cond(block_start < last_pos, compute, keep_state, running_state), None)

    running, unused = lax.scan(
        one_block, running, (key_blocks, value_blocks, gate_blocks, block_starts)
    )
    highest, totals, weighted = running
    return (weighted / totals.T[:, :, None]).reshape(length, row_width).astype(jnp.bfloat16)


def body(
    queries,
    key_rows,
    value_rows,
    log_forget,
    stream_in,
    out_weight,
    mix_gain,
    mix_bias,
    gate_weight,
    up_weight,
    down_weight,
    ffn_gain,
    ffn_bias,
):
    attended = attend(queries, key_rows, value_rows, log_forget)
    length = attended.shape[0]
    own_rows = length // lax.axis_size("tp")
    offset = lax.axis_index("tp") * own_rows
    summed = lax.psum_scatter(
        jnp.dot(attended, out_weight, preferred_element_type=jnp.float32).astype(jnp.bfloat16),
        "tp",
        scatter_dimension=0,
        tiled=True,
    )
    mix_out = lax.optimization_barrier(summed).astype(jnp.float32)
    stream_own = lax.dynamic_slice_in_dim(stream_in, offset, own_rows, 0)
    normed = layer_norm(
        ALPHA * stream_own.astype(jnp.float32) + mix_out, mix_gain, mix_bias
    ).astype(jnp.bfloat16)
    gathered = lax.all_gather(normed, "tp", axis=0, tiled=True)
    gate_part = jnp.dot(
        gathered,
        lax.all_gather(gate_weight, "sp", axis=0, tiled=True),
        preferred_element_type=jnp.float32,
    )
    up_part = jnp.dot(
        gathered,
        lax.all_gather(up_weight, "sp", axis=0, tiled=True),
        preferred_element_type=jnp.float32,
    )
    hidden = (jax.nn.silu(gate_part) * up_part).astype(jnp.bfloat16)
    partial_terms = jnp.dot(
        hidden,
        lax.all_gather(down_weight, "sp", axis=1, tiled=True),
        preferred_element_type=jnp.float32,
    )
    lowered = lax.psum_scatter(
        partial_terms.astype(jnp.bfloat16), "tp", scatter_dimension=0, tiled=True
    ).astype(jnp.float32)
    lowered = lax.optimization_barrier(lowered.astype(jnp.bfloat16)).astype(jnp.float32)
    result = layer_norm(ALPHA * normed.astype(jnp.float32) + lowered, ffn_gain, ffn_bias)
    return result.astype(jnp.bfloat16)


def solution(mesh):
    placed = (
        P("sp", "tp"),
        P("sp", "tp"),
        P("sp", "tp"),
        P("sp", "tp"),
        P("sp", None),
        P("tp", None),
        P(),
        P(),
        P("sp", "tp"),
        P("sp", "tp"),
        P("tp", "sp"),
        P(),
        P(),
    )
    return jax.shard_map(
        body, mesh=mesh, in_specs=placed, out_specs=P(("sp", "tp"), None), check_vma=False
    )
```

profile of v0, /device:TPU:0, one launch (start us, length us, event | category | flops | bytes accessed | tf_op | source)
XLA Modules:
  0.0 859.3 jit_solution(4486789846693739934)
XLA Ops:
  6.5 0.0 copy-start
  6.5 0.0 all-gather.7.cloned.1.call-start
  6.5 0.7 all-gather.7.cloned.1.call-update
  7.3 0.0 all-gather.9.cloned.1.call-start
  7.3 0.7 all-gather.9.cloned.1.call-update
  8.0 0.0 reduce-scatter.3.cloned.1.call-start
  8.1 1.4 copy.18
  9.5 0.0 copy-done.6
  9.5 35.9 %all_gather.22 = f32[6144,8]{0,1:T(8,128)} all-gather(f32[768,8]{0,1:T(8,128)S(1)} %copy-done.6), channel_id=1, replica_groups=mesh['sp'=8,'tp'=4] {'sp'}, dimensions={0}, use_global_device_ids=true | all-gather | bytes 221184 | tf_op jit(solution)/shard_map/all_gather | solution.py:26
  45.4 66.8 %all-gather.7.cloned.1.call-done = bf16[6144,512]{1,0:T(8,128)(2,1)} async-done(((bf16[768,512]{1,0:T(8,128)(2,1)}), bf16[6144,512]{1,0:T(8,128)(2,1)}) %all-gather.7.cloned.1.call-update) | async-done | bytes 6291472 | tf_op jit(solution)/shard_map/all_gather | solution.py:33
  112.2 16.3 %reshape.82 = bf16[8,768,8,64]{3,2,1,0:T(8,128)(2,1)} reshape(bf16[6144,512]{1,0:T(8,128)(2,1)} %all-gather.7.cloned.1.call-done) | data formatting | bytes 12582912 | tf_op jit(solution)/shard_map/reshape | solution.py:46
  128.4 13.3 %copy.20 = bf16[8,768,8,64]{1,3,2,0:T(8,128)(2,1)} copy(bf16[8,768,8,64]{3,2,1,0:T(8,128)(2,1)} %reshape.82) | data formatting | bytes 12582912
  141.7 69.5 %all-gather.9.cloned.1.call-done = bf16[6144,512]{1,0:T(8,128)(2,1)} async-done(((bf16[768,512]{1,0:T(8,128)(2,1)}), bf16[6144,512]{1,0:T(8,128)(2,1)}) %all-gather.9.cloned.1.call-update) | async-done | bytes 6291472 | tf_op jit(solution)/shard_map/all_gather | solution.py:34
  211.2 16.2 %reshape.83 = bf16[8,768,8,64]{3,2,1,0:T(8,128)(2,1)} reshape(bf16[6144,512]{1,0:T(8,128)(2,1)} %all-gather.9.cloned.1.call-done) | data formatting | bytes 12582912 | tf_op jit(solution)/shard_map/reshape | solution.py:47
  227.5 13.2 %copy.21 = bf16[8,768,8,64]{1,3,2,0:T(8,128)(2,1)} copy(bf16[8,768,8,64]{3,2,1,0:T(8,128)(2,1)} %reshape.83) | data formatting | bytes 12582912
  240.6 1.3 broadcast_in_dim.52
  242.0 34.5 %while.15 = (s32[]{:T(128)}, f32[8,768]{1,0:T(8,128)S(1)}, f32[8,768]{1,0:T(8,128)S(1)}, f32[768,8,64]{0,2,1:T(8,128)}, s32[8]{0:T(128)S(1)}, /*index=5*/s32[]{:...) while((s32[]{:T(128)}, f32[8,768]{1,0:T(8,128)S(1)}, ...), condition=%wide.region_5.6_spmd.clone, body=%wide.region_0.5_spmd.clone.sunk | while | flops 1299009024 | bytes 77679992 | solution.py:83
  242.0 0.6 dynamic_slice.50
  243.2 23.8 %conditional.3 = ((f32[8,768]{1,0:T(8,128)S(1)}, f32[8,768]{1,0:T(8,128)S(1)}, f32[768,8,64]{0,2,1:T(8,128)})) conditional(s32[]{:T(128)} %convert_element_type.96, (f32[8,768]{1,0:T(8,128)S(1)}, f32[8,768]{1,0:T(8,128)S(1)}, f32[768,8,64]{0,2,1:T(8,128)}) %tuple.40, (s32[]{:T(128)}, s32[]{:T(128)}, bf16[8,768,8,64]{1,3,2,0:T(8,128)(2,1)}, s32[]{:T(128)}, ...), branch_computations={%region_1.1_spmd, %region_2.4_spmd} | conditional | flops 1299009024 | bytes 77676648 | solution.py:81
  243.2 0.6 iota_add_fusion
  243.9 0.4 broadcast_compare_fusion
  244.3 0.7 dynamic-slice_bitcast_fusion
  245.0 6.6 fusion.4
  251.6 0.0 copy-done.4
  251.7 8.0 bitcast_add_fusion
  259.7 0.0 copy-start.5
  259.7 7.3 fusion.3
  267.0 0.0 copy-done.5
  267.1 0.6 dynamic_slice.50
  268.4 0.6 dynamic_slice.50
  269.7 0.6 dynamic_slice.50
  271.0 0.6 dynamic_slice.50
  272.3 0.6 dynamic_slice.50
  273.6 0.6 dynamic_slice.50
  274.9 0.6 dynamic_slice.50
  276.4 1.5 divide_convert_fusion
  278.0 0.0 copy-done
  278.0 3.5 convolution_convert_fusion
  281.5 0.0 reduce-scatter.3.cloned.1.call-update
  281.6 0.0 all-gather.13.cloned.1.call-start
  281.6 0.5 all-gather.13.cloned.1.call-update
  282.1 0.0 all-gather.11.cloned.1.call-start
  282.2 202.4 %reduce-scatter.3.cloned.1.call-done = bf16[192,2048]{1,0:T(8,128)(2,1)} async-done(((bf16[768,2048]{1,0:T(8,128)(2,1)}), bf16[192,2048]{1,0:T(8,128)(2,1)}) %reduce-scatter.3.cloned.1.call-update) | async-done | bytes 786448 | tf_op jit(solution)/shard_map/reduce_scatter | solution.py:109
  484.6 1.8 fusion.21
  486.4 1.8 multiply_reduce_fusion.1
  488.2 2.5 add_convert_fusion.1
  490.7 0.0 all-gather.11.cloned.1.call-update
  490.8 0.0 all-gather.15.cloned.1.call-start
  490.8 0.5 all-gather.15.cloned.1.call-update
  491.3 0.0 all-gather.17.cloned.1.call-start
  491.4 0.7 all-gather.17.cloned.1.call-update
  492.1 0.0 reduce-scatter.5.cloned.1.call-start
  492.1 86.8 %all-gather.13.cloned.1.call-done = bf16[2048,1408]{1,0:T(8,128)(2,1)} async-done(((bf16[256,1408]{1,0:T(8,128)(2,1)}), bf16[2048,1408]{1,0:T(8,128)(2,1)}) %all-gather.13.cloned.1.call-update) | async-done | bytes 5767184 | tf_op jit(solution)/shard_map/all_gather | solution.py:123
  579.0 28.1 %all-gather.11.cloned.1.call-done = bf16[768,2048]{1,0:T(8,128)(2,1)} async-done(((bf16[192,2048]{1,0:T(8,128)(2,1)}), bf16[768,2048]{1,0:T(8,128)(2,1)}) %all-gather.11.cloned.1.call-update) | async-done | bytes 3145744 | tf_op jit(solution)/shard_map/all_gather | solution.py:120
  607.1 9.7 %fusion.24 = f32[768,1408]{1,0:T(8,128)} fusion(bf16[768,2048]{1,0:T(8,128)(2,1)} %all-gather.11.cloned.1.call-done, bf16[2048,1408]{1,0:T(8,128)(2,1)} %all-gather.13.cloned.1.call-done), kind=kOutput, calls=%fused_computation.44 | convolution fusion | flops 4429185024 | bytes 13238272 | tf_op jit(solution)/shard_map/dot_general | solution.py:121
  616.8 84.7 %all-gather.15.cloned.1.call-done = bf16[2048,1408]{1,0:T(8,128)(2,1)} async-done(((bf16[256,1408]{1,0:T(8,128)(2,1)}), bf16[2048,1408]{1,0:T(8,128)(2,1)}) %all-gather.15.cloned.1.call-update) | async-done | bytes 5767184 | tf_op jit(solution)/shard_map/all_gather | solution.py:128
  701.5 93.4 %all-gather.17.cloned.1.call-done = bf16[1408,2048]{1,0:T(8,128)(2,1)} async-done(((bf16[1408,256]{1,0:T(8,128)(2,1)}), bf16[1408,2048]{1,0:T(8,128)(2,1)}) %all-gather.17.cloned.1.call-update) | async-done | bytes 5767184 | tf_op jit(solution)/shard_map/all_gather | solution.py:134
  794.9 16.8 %convolution_convert_fusion.1 = bf16[768,2048]{1,0:T(8,128)(2,1)} fusion(bf16[1408,2048]{1,0:T(8,128)(2,1)} %all-gather.17.cloned.1.call-done, f32[768,1408]{1,0:T(8,128)} %fusion.24, bf16[768,2048]{1,0:T(8,128)(2,1)} %all-gather.11.cloned.1.call-done, bf16[2048,1408]{1,0:T(8,128)(2,1)} %all-gather.15.cloned.1.call-done), kind=kOutput, calls=%fused_computation.28 | convolution fusion | flops 8866430976 | bytes 22151168 | tf_op jit(solution)/shard_map/dot_general | solution.py:132
  811.7 0.0 reduce-scatter.5.cloned.1.call-update
  811.7 36.2 %reduce-scatter.5.cloned.1.call-done = bf16[192,2048]{1,0:T(8,128)(2,1)} async-done(((bf16[768,2048]{1,0:T(8,128)(2,1)}), bf16[192,2048]{1,0:T(8,128)(2,1)}) %reduce-scatter.5.cloned.1.call-update) | async-done | bytes 786448 | tf_op jit(solution)/shard_map/reduce_scatter | solution.py:137
  847.9 1.5 fusion.22
  849.5 1.6 multiply_reduce_fusion
  851.0 0.0 copy-done.9
  851.1 1.3 add_convert_fusion
  (40 shorter events, 0.2 us)
Async XLA Ops:
  6.5 271.4 %copy-start = (bf16[512,2048]{1,0:T(8,128)(2,1)S(1)}, bf16[512,2048]{1,0:T(8,128)(2,1)}, u32[]{:S(2)}) copy-start(bf16[512,2048]{1,0:T(8,128)(2,1)} %param.22) | copy-start | bytes 6291460
  6.5 2.9 copy-start.6
  6.5 105.6 %all-gather.7.cloned.1.call-start = ((), (), s32[]{:S(2)}) async-start(), calls=%async_computation.2 | async-start | bytes 7077888 | tf_op jit(solution)/shard_map/all_gather | solution.py:33
  7.3 204.0 %all-gather.9.cloned.1.call-start = ((), (), s32[]{:S(2)}) async-start(), calls=%async_computation.3 | async-start | bytes 7077888 | tf_op jit(solution)/shard_map/all_gather | solution.py:34
  8.0 476.6 %reduce-scatter.3.cloned.1.call-start = ((), (), s32[]{:S(2)}) async-start(), calls=%async_computation.4 | async-start | bytes 3932160 | tf_op jit(solution)/shard_map/reduce_scatter | solution.py:109
  245.0 6.6 copy-start.4
  259.7 7.4 copy-start.5
  281.5 206.7 %copy-start.7 = (f32[2048]{0:T(1024)S(1)}, f32[2048]{0:T(1024)}, u32[]{:S(2)}) copy-start(f32[2048]{0:T(1024)} %param.24) | copy-start | bytes 24580
  281.5 206.7 %copy-start.8 = (f32[2048]{0:T(1024)S(1)}, f32[2048]{0:T(1024)}, u32[]{:S(2)}) copy-start(f32[2048]{0:T(1024)} %param.23) | copy-start | bytes 24580
  281.6 297.4 %all-gather.13.cloned.1.call-start = ((), (), s32[]{:S(2)}) async-start(), calls=%async_computation.6 | async-start | bytes 6488064 | tf_op jit(solution)/shard_map/all_gather | solution.py:123
  282.1 325.0 %all-gather.11.cloned.1.call-start = ((), (), s32[]{:S(2)}) async-start(), calls=%async_computation.5 | async-start | bytes 3932160 | tf_op jit(solution)/shard_map/all_gather | solution.py:120
  484.6 3.6 copy-start.2
  490.8 210.7 %all-gather.15.cloned.1.call-start = ((), (), s32[]{:S(2)}) async-start(), calls=%async_computation.7 | async-start | bytes 6488064 | tf_op jit(solution)/shard_map/all_gather | solution.py:128
  491.3 303.5 %all-gather.17.cloned.1.call-start = ((), (), s32[]{:S(2)}) async-start(), calls=%async_computation.8 | async-start | bytes 6488064 | tf_op jit(solution)/shard_map/all_gather | solution.py:134
  492.1 355.8 %reduce-scatter.5.cloned.1.call-start = ((), (), s32[]{:S(2)}) async-start(), calls=%async_computation.9 | async-start | bytes 3932160 | tf_op jit(solution)/shard_map/reduce_scatter | solution.py:137
  811.6 36.3 %copy-start.1 = (bf16[192,2048]{1,0:T(8,128)(2,1)S(1)}, bf16[192,2048]{1,0:T(8,128)(2,1)}, u32[]{:S(2)}) copy-start(bf16[192,2048]{1,0:T(8,128)(2,1)} %add_convert_fusion.1) | copy-start | bytes 2359300
  811.6 39.4 %copy-start.9 = (f32[2048]{0:T(1024)S(1)}, f32[2048]{0:T(1024)}, u32[]{:S(2)}) copy-start(f32[2048]{0:T(1024)} %param.29) | copy-start | bytes 24580
  811.6 39.4 %copy-start.10 = (f32[2048]{0:T(1024)S(1)}, f32[2048]{0:T(1024)}, u32[]{:S(2)}) copy-start(f32[2048]{0:T(1024)} %param.28) | copy-start | bytes 24580
  847.9 3.2 copy-start.3
Sparse Core Ops, SparseCore 0:
  9.5 102.5 all-gather.6
  114.3 96.8 all-gather.8
  281.7 202.8 reduce-scatter.2
  486.6 92.2 all-gather.12
  580.4 26.6 all-gather.10
  609.1 92.3 all-gather.14
  703.5 91.2 all-gather.16
  811.8 36.0 reduce-scatter.4
where the time goes:
time: 862 us; the launch traced here: 859 us
  waiting for transfers between devices  671 us (78%)
  local copies, waits for them, and re-layouts  67.6 us (8%)
  matrix products  44.6 us (5%)
  blocking collectives  35.9 us (4%)
  other arithmetic  20.5 us (2%)
  between operations  13.6 us (2%)
    reduce_scatter x1, waiting for transfers between devices, body(): lax.psum_scatter(jnp.dot(attended, out_weight, preferred_element_type=jnp...  202 us
    all_gather x1, waiting for transfers between devices, body(): lax.all_gather(down_weight, 'sp', axis=1, tiled=True)  93.4 us
    all_gather x1, waiting for transfers between devices, body(): lax.all_gather(gate_weight, 'sp', axis=0, tiled=True)  86.8 us
    all_gather x1, waiting for transfers between devices, body(): lax.all_gather(up_weight, 'sp', axis=0, tiled=True)  84.7 us
    all_gather x1, waiting for transfers between devices, attend(): value_piece = lax.all_gather(value_rows, 'sp', axis=0, tiled=True)  69.5 us
    all_gather x1, waiting for transfers between devices, attend(): key_piece = lax.all_gather(key_rows, 'sp', axis=0, tiled=True)  66.8 us
    reduce_scatter x1, waiting for transfers between devices, body(): lax.psum_scatter(partial_terms.astype(jnp.bfloat16), 'tp', scatter_dimens...  36.2 us
    all_gather x1, blocking collectives, attend(): gates_all = lax.all_gather(log_forget, 'sp', axis=0, tiled=True)  35.9 us
  transfers between devices with their start and end apart: 8, of which 8 were waited for; matrix products, arithmetic and copies ran while one was open for 5% of the time, Pallas kernels for 0%

commit v1 on v0

--- a/solution.py
+++ b/solution.py
@@ -1,6 +1,8 @@
 import jax
 import jax.numpy as jnp
 from jax import lax
+from jax.experimental import pallas as pl
+from jax.experimental.pallas import tpu as pltpu
 from jax.sharding import PartitionSpec as P
 
 ALPHA = 8.0**0.25
@@ -87,6 +89,110 @@
     return (weighted / totals.T[:, :, None]).reshape(length, row_width).astype(jnp.bfloat16)
 
 
+SUB = 256
+
+
+def flash_kernel(packed_ref, out_ref, query_ref, value_ref, high_ref, acc_ref):
+    pieces, rows, length = packed_ref.shape
+    head_dim = out_ref.shape[1]
+    sub = SUB if length % SUB == 0 else length
+    gate_rows = rows - 3 * head_dim
+    query_at = head_dim + gate_rows
+    value_at = query_at + head_dim
+    tail = jnp.zeros((128 - head_dim - gate_rows, length), jnp.bfloat16)
+    row_index = lax.broadcasted_iota(jnp.int32, (gate_rows, length), 0)
+    minus = jnp.where(row_index < 3, -1.0, 0.0).astype(jnp.bfloat16)
+    ones = jnp.where(row_index < 1, 1.0, 0.0).astype(jnp.bfloat16)
+    scale = head_dim**-0.5
+
+    def set_values(piece, carry):
+        block = packed_ref[piece, value_at : value_at + head_dim, :]
+        value_ref[piece] = jnp.concatenate([block, ones, tail], axis=0).T
+        return carry
+
+    lax.fori_loop(0, pieces, set_values, 0)
+
+    def pair(piece, diagonal):
+        key_block = packed_ref[piece, 0:128, :]
+        for start in range(0, length, sub):
+            width = min(length, start + sub) if diagonal else length
+            keys = key_block[:, :width]
+            scores = jnp.dot(
+                query_ref[start : start + sub, :], keys, preferred_element_type=jnp.float32
+            )
+            if diagonal:
+                key_pos = lax.broadcasted_iota(jnp.int32, (sub, width), 1)
+                query_pos = start + lax.broadcasted_iota(jnp.int32, (sub, width), 0)
+                scores = jnp.where(key_pos <= query_pos, scores, -1e30)
+            old_high = high_ref[start : start + sub, :]
+            new_high = jnp.maximum(old_high, jnp.max(scores, axis=1, keepdims=True))
+            weights = jnp.exp(scores - new_high[:, :1]).astype(jnp.bfloat16)
+            factor = jnp.exp(old_high - new_high)
+            high_ref[start : start + sub, :] = new_high
+            acc_ref[start : start + sub, :] = acc_ref[start : start + sub, :] * factor + jnp.dot(
+                weights, value_ref[piece, :width, :], preferred_element_type=jnp.float32
+            )
+
+    def one_query_piece(index, carry):
+        block = packed_ref[index, query_at : query_at + head_dim, :]
+        scaled = (block.astype(jnp.float32) * scale).astype(jnp.bfloat16)
+        query_ref[...] = jnp.concatenate([scaled, minus, tail], axis=0).T
+        high_ref[...] = jnp.full_like(high_ref, -1e30)
+        acc_ref[...] = jnp.zeros_like(acc_ref)
+
+        def earlier(piece, inner):
+            pair(piece, False)
+            return inner
+
+        lax.fori_loop(0, index, earlier, 0)
+        pair(index, True)
+        turned = acc_ref[...].T
+        out_ref[index] = (turned[:head_dim] / turned[head_dim : head_dim + 1]).astype(jnp.bfloat16)
+        return carry
+
+    lax.fori_loop(0, pieces, one_query_piece, 0)
+
+
+def attend_by_head(queries, key_rows, value_rows, log_forget):
+    length, row_width = queries.shape
+    heads = log_forget.shape[1]
+    head_dim = row_width // heads
+    pieces = lax.axis_size("sp")
+
+    def turn(matrix):
+        return matrix.T.reshape(heads, head_dim, length)
+
+    gates = log_forget.T
+    high = lax.reduce_precision(gates, 8, 7)
+    middle = lax.reduce_precision(gates - high, 8, 7)
+    low = gates - high - middle
+    gate_rows = jnp.stack([high, middle, low], axis=1).astype(jnp.bfloat16)
+    gate_rows = jnp.pad(gate_rows, ((0, 0), (0, 13), (0, 0)))
+    packed = jnp.concatenate(
+        [turn(key_rows), gate_rows, turn(queries), turn(value_rows)], axis=1
+    )
+    packed = lax.all_to_all(packed, "sp", 0, 0, tiled=True)
+    flops = 2 * pieces * pieces * length * length * 128
+    attended = pl.pallas_call(
+        flash_kernel,
+        out_shape=jax.ShapeDtypeStruct((pieces, head_dim, length), jnp.bfloat16),
+        in_specs=[pl.BlockSpec(memory_space=pltpu.VMEM)],
+        out_specs=pl.BlockSpec(memory_space=pltpu.VMEM),
+        scratch_shapes=[
+            pltpu.VMEM((length, 128), jnp.bfloat16),
+            pltpu.VMEM((pieces, length, 128), jnp.bfloat16),
+            pltpu.VMEM((length, 128), jnp.float32),
+            pltpu.VMEM((length, 128), jnp.float32),
+        ],
+        compiler_params=pltpu.CompilerParams(vmem_limit_bytes=40 * 1024 * 1024),
+        cost_estimate=pl.CostEstimate(
+            flops=4 * flops, bytes_accessed=packed.size * 2, transcendentals=0
+        ),
+    )(packed)
+    back = lax.all_to_all(attended, "sp", 0, 0, tiled=True)
+    return back.reshape(row_width, length)
+
+
 def body(
     queries,
     key_rows,
@@ -102,12 +208,23 @@
     ffn_gain,
     ffn_bias,
 ):
-    attended = attend(queries, key_rows, value_rows, log_forget)
-    length = attended.shape[0]
+    length = queries.shape[0]
+    heads = log_forget.shape[1]
+    head_dim = queries.shape[1] // heads
+    by_head = heads == lax.axis_size("sp") and head_dim + 16 <= 128 and head_dim % 16 == 0
+    if by_head:
+        turned = attend_by_head(queries, key_rows, value_rows, log_forget)
+    else:
+        turned = attend(queries, key_rows, value_rows, log_forget).T
     own_rows = length // lax.axis_size("tp")
     offset = lax.axis_index("tp") * own_rows
     summed = lax.psum_scatter(
-        jnp.dot(attended, out_weight, preferred_element_type=jnp.float32).astype(jnp.bfloat16),
+        lax.dot_general(
+            turned,
+            out_weight,
+            (((0,), (0,)), ((), ())),
+            preferred_element_type=jnp.float32,
+        ).astype(jnp.bfloat16),
         "tp",
         scatter_dimension=0,
         tiled=True,

time: 862 us -> 545 us (0.63)
  waiting for transfers between devices: 671 us -> 329 us
  Pallas kernels: 0 us -> 62 us
  local copies, waits for them, and re-layouts: 67.6 us -> 6.08 us
  blocking collectives: 35.9 us -> 88.4 us
  matrix products: 44.6 us -> 30 us
    reduce_scatter x1, waiting for transfers between devices: 202 us -> 36.4 us  [body(): lax.psum_scatter(lax.dot_general(turned, out_weight, (((0,), (0,)), ((),...]
    all_gather x2 -> x0, waiting for transfers between devices: 136 us -> none  [the longest x1 69.5 us: attend(): value_piece = lax.all_gather(value_rows, 'sp', axis=0, tiled=True)]
    all_to_all x0 -> x2, blocking collectives: none -> 88.4 us  [the longest x1 65.2 us: attend_by_head(): packed = lax.all_to_all(packed, 'sp', 0, 0, tiled=True)]
    pallas_call x0 -> x1, Pallas kernels: none -> 62 us  [attend_by_head(): pl.pallas_call(flash_kernel, out_shape=jax.ShapeDtypeStruct((pieces, head...]
    all_gather x1, waiting for transfers between devices: 86.8 us -> 49.1 us  [body(): lax.all_gather(gate_weight, 'sp', axis=0, tiled=True)]
    all_gather x1 -> x0, blocking collectives: 35.9 us -> none  [attend(): gates_all = lax.all_gather(log_forget, 'sp', axis=0, tiled=True)]
    reshape x2 -> x0, local copies, waits for them, and re-layouts: 32.5 us -> none  [the longest x1 16.3 us: attend(): key_blocks = key_piece.reshape(blocks, block_len, head_count, head_dim)]
    unnamed x21 -> x16, local copies, waits for them, and re-layouts: 27.9 us -> 0.04 us
  transfers between devices with their start and end apart: 8 -> 6, of which waited for: 8 -> 6; matrix products, arithmetic and copies ran while one was open for 5% -> 3% of each run, Pallas kernels for 0% -> 0%
where the time goes in v1:
time: 545 us; the launch traced here: 544 us
  waiting for transfers between devices  329 us (60%)
  blocking collectives  88.4 us (16%)
  Pallas kernels  62 us (11%)
  matrix products  30 us (6%)
  between operations  15.2 us (3%)
  other arithmetic  13.1 us (2%)
  local copies, waits for them, and re-layouts  6.08 us (1%)
    all_gather x1, waiting for transfers between devices, body(): lax.all_gather(up_weight, 'sp', axis=0, tiled=True)  92.5 us
    all_gather x1, waiting for transfers between devices, body(): lax.all_gather(down_weight, 'sp', axis=1, tiled=True)  85.2 us
    all_to_all x1, blocking collectives, attend_by_head(): packed = lax.all_to_all(packed, 'sp', 0, 0, tiled=True)  65.2 us
    pallas_call x1, Pallas kernels, attend_by_head(): pl.pallas_call(flash_kernel, out_shape=jax.ShapeDtypeStruct((pieces, head...  62 us
    all_gather x1, waiting for transfers between devices, body(): lax.all_gather(gate_weight, 'sp', axis=0, tiled=True)  49.1 us
    reduce_scatter x1, waiting for transfers between devices, body(): lax.psum_scatter(lax.dot_general(turned, out_weight, (((0,), (0,)), ((),...  36.4 us
    reduce_scatter x1, waiting for transfers between devices, body(): lax.psum_scatter(partial_terms.astype(jnp.bfloat16), 'tp', scatter_dimens...  36.1 us
    all_gather x1, waiting for transfers between devices, body(): gathered = lax.all_gather(normed, 'tp', axis=0, tiled=True)  28 us
  transfers between devices with their start and end apart: 6, of which 6 were waited for; matrix products, arithmetic and copies ran while one was open for 3% of the time, Pallas kernels for 0%

profile of v1, /device:TPU:0, one launch (start us, length us, event | category | flops | bytes accessed | tf_op | source)
XLA Modules:
  0.0 544.3 jit_solution(830724791563535705)
XLA Ops:
  7.4 0.0 copy-start
  7.4 0.0 reduce-scatter.3.cloned.1.call-start
  7.4 0.9 fusion.9
  8.3 1.4 copy.29
  9.8 2.3 copy.33
  12.1 2.3 copy.34
  14.3 0.1 fusion.6
  14.4 1.5 pad_maximum_fusion
  15.9 65.2 %all_to_all.10.packed_ref = bf16[8,208,768]{2,1,0:T(8,128)(2,1)S(1)} all-to-all(bf16[8,208,768]{2,1,0:T(8,128)(2,1)S(1)} %pad_maximum_fusion), channel_id=1, replica_groups=mesh['sp'=8,'tp'=4] {'sp'}, dimensions={0} | all-to-all | bytes 5111808 | tf_op jit(solution)/shard_map/all_to_all | solution.py:174
  81.2 62.0 %shard_map.127 = bf16[8,64,768]{2,1,0:T(8,128)(2,1)S(1)} custom-call(bf16[8,208,768]{2,1,0:T(8,128)(2,1)S(1)} %all_to_all.10.packed_ref), custom_call_target="tpu_custom_call" | custom-call | flops 38654705664 | bytes 2555904 | tf_op jit(solution)/shard_map/pallas_call | solution.py:176
  143.2 23.2 %all_to_all.11 = bf16[8,64,768]{2,1,0:T(8,128)(2,1)S(1)} all-to-all(bf16[8,64,768]{2,1,0:T(8,128)(2,1)S(1)} %shard_map.127), channel_id=1, replica_groups=mesh['sp'=8,'tp'=4] {'sp'}, dimensions={0} | all-to-all | bytes 1572864 | tf_op jit(solution)/shard_map/all_to_all | solution.py:192
  166.4 0.0 copy-done
  166.4 3.6 convolution_convert_fusion
  170.0 0.0 reduce-scatter.3.cloned.1.call-update
  170.0 0.0 copy-start.4
  170.0 0.0 copy-start.5
  170.0 0.0 all-gather.7.cloned.1.call-start
  170.1 0.5 all-gather.7.cloned.1.call-update
  170.6 0.0 all-gather.5.cloned.1.call-start
  170.6 36.4 %reduce-scatter.3.cloned.1.call-done = bf16[192,2048]{1,0:T(8,128)(2,1)} async-done(((bf16[768,2048]{1,0:T(8,128)(2,1)}), bf16[192,2048]{1,0:T(8,128)(2,1)}) %reduce-scatter.3.cloned.1.call-update) | async-done | bytes 786448 | tf_op jit(solution)/shard_map/reduce_scatter | solution.py:221
  207.0 0.0 copy-start.2
  207.1 1.8 fusion
  208.8 1.8 multiply_reduce_fusion.1
  210.7 0.0 copy-done.4
  210.7 0.0 copy-done.5
  210.7 0.0 copy-done.2
  210.7 2.5 add_convert_fusion.1
  213.2 0.0 all-gather.5.cloned.1.call-update
  213.2 0.0 all-gather.11.cloned.1.call-start
  213.3 0.5 all-gather.11.cloned.1.call-update
  213.8 0.0 all-gather.9.cloned.1.call-start
  213.8 0.7 all-gather.9.cloned.1.call-update
  214.5 0.2 reduce-scatter.5.cloned.1.call-start
  214.8 49.1 %all-gather.7.cloned.1.call-done = bf16[2048,1408]{1,0:T(8,128)(2,1)} async-done(((bf16[256,1408]{1,0:T(8,128)(2,1)}), bf16[2048,1408]{1,0:T(8,128)(2,1)}) %all-gather.7.cloned.1.call-update) | async-done | bytes 5767184 | tf_op jit(solution)/shard_map/all_gather | solution.py:240
  263.9 28.0 %all-gather.5.cloned.1.call-done = bf16[768,2048]{1,0:T(8,128)(2,1)} async-done(((bf16[192,2048]{1,0:T(8,128)(2,1)}), bf16[768,2048]{1,0:T(8,128)(2,1)}) %all-gather.5.cloned.1.call-update) | async-done | bytes 3145744 | tf_op jit(solution)/shard_map/all_gather | solution.py:237
  291.8 9.7 %fusion.12 = f32[768,1408]{1,0:T(8,128)} fusion(bf16[768,2048]{1,0:T(8,128)(2,1)} %all-gather.5.cloned.1.call-done, bf16[2048,1408]{1,0:T(8,128)(2,1)} %all-gather.7.cloned.1.call-done), kind=kOutput, calls=%fused_computation.31 | convolution fusion | flops 4429185024 | bytes 13238272 | tf_op jit(solution)/shard_map/dot_general | solution.py:238
  301.5 85.2 %all-gather.11.cloned.1.call-done = bf16[1408,2048]{1,0:T(8,128)(2,1)} async-done(((bf16[1408,256]{1,0:T(8,128)(2,1)}), bf16[1408,2048]{1,0:T(8,128)(2,1)}) %all-gather.11.cloned.1.call-update) | async-done | bytes 5767184 | tf_op jit(solution)/shard_map/all_gather | solution.py:251
  386.7 92.5 %all-gather.9.cloned.1.call-done = bf16[2048,1408]{1,0:T(8,128)(2,1)} async-done(((bf16[256,1408]{1,0:T(8,128)(2,1)}), bf16[2048,1408]{1,0:T(8,128)(2,1)}) %all-gather.9.cloned.1.call-update) | async-done | bytes 5767184 | tf_op jit(solution)/shard_map/all_gather | solution.py:245
  479.2 16.8 %convolution_convert_fusion.1 = bf16[768,2048]{1,0:T(8,128)(2,1)} fusion(bf16[1408,2048]{1,0:T(8,128)(2,1)} %all-gather.11.cloned.1.call-done, f32[768,1408]{1,0:T(8,128)} %fusion.12, bf16[768,2048]{1,0:T(8,128)(2,1)} %all-gather.5.cloned.1.call-done, bf16[2048,1408]{1,0:T(8,128)(2,1)} %all-gather.9.cloned.1.call-done), kind=kOutput, calls=%fused_computation.2 | convolution fusion | flops 8866430976 | bytes 22151168 | tf_op jit(solution)/shard_map/dot_general | solution.py:249
  496.0 0.0 copy-start.1
  496.0 0.0 reduce-scatter.5.cloned.1.call-update
  496.0 0.0 copy-start.6
  496.0 0.0 copy-start.7
  496.0 36.1 %reduce-scatter.5.cloned.1.call-done = bf16[192,2048]{1,0:T(8,128)(2,1)} async-done(((bf16[768,2048]{1,0:T(8,128)(2,1)}), bf16[192,2048]{1,0:T(8,128)(2,1)}) %reduce-scatter.5.cloned.1.call-update) | async-done | bytes 786448 | tf_op jit(solution)/shard_map/reduce_scatter | solution.py:254
  532.2 0.0 copy-done.1
  532.2 0.0 copy-start.3
  532.2 1.5 fusion.1
  533.7 1.6 multiply_reduce_fusion
  535.3 0.0 copy-done.6
  535.3 0.0 copy-done.7
  535.3 0.0 copy-done.3
  535.3 1.3 add_convert_fusion
  (7 shorter events, 0.1 us)
Async XLA Ops:
  7.4 159.0 %copy-start = (bf16[512,2048]{1,0:T(8,128)(2,1)S(1)}, bf16[512,2048]{1,0:T(8,128)(2,1)}, u32[]{:S(2)}) copy-start(bf16[512,2048]{1,0:T(8,128)(2,1)} %param.18) | copy-start | bytes 6291460
  7.4 199.7 %reduce-scatter.3.cloned.1.call-start = ((), (), s32[]{:S(2)}) async-start(), calls=%async_computation.4 | async-start | bytes 3932160 | tf_op jit(solution)/shard_map/reduce_scatter | solution.py:221
  170.0 40.7 %copy-start.4 = (f32[2048]{0:T(1024)S(1)}, f32[2048]{0:T(1024)}, u32[]{:S(2)}) copy-start(f32[2048]{0:T(1024)} %param.20) | copy-start | bytes 24580
  170.0 40.7 %copy-start.5 = (f32[2048]{0:T(1024)S(1)}, f32[2048]{0:T(1024)}, u32[]{:S(2)}) copy-start(f32[2048]{0:T(1024)} %param.19) | copy-start | bytes 24580
  170.0 93.8 %all-gather.7.cloned.1.call-start = ((), (), s32[]{:S(2)}) async-start(), calls=%async_computation.6 | async-start | bytes 6488064 | tf_op jit(solution)/shard_map/all_gather | solution.py:240
  170.6 121.2 %all-gather.5.cloned.1.call-start = ((), (), s32[]{:S(2)}) async-start(), calls=%async_computation.5 | async-start | bytes 3932160 | tf_op jit(solution)/shard_map/all_gather | solution.py:237
  207.0 3.6 copy-start.2
  213.2 173.4 %all-gather.11.cloned.1.call-start = ((), (), s32[]{:S(2)}) async-start(), calls=%async_computation.8 | async-start | bytes 6488064 | tf_op jit(solution)/shard_map/all_gather | solution.py:251
  213.8 265.4 %all-gather.9.cloned.1.call-start = ((), (), s32[]{:S(2)}) async-start(), calls=%async_computation.7 | async-start | bytes 6488064 | tf_op jit(solution)/shard_map/all_gather | solution.py:245
  214.5 317.6 %reduce-scatter.5.cloned.1.call-start = ((), (), s32[]{:S(2)}) async-start(), calls=%async_computation.9 | async-start | bytes 3932160 | tf_op jit(solution)/shard_map/reduce_scatter | solution.py:254
  496.0 36.2 %copy-start.1 = (bf16[192,2048]{1,0:T(8,128)(2,1)S(1)}, bf16[192,2048]{1,0:T(8,128)(2,1)}, u32[]{:S(2)}) copy-start(bf16[192,2048]{1,0:T(8,128)(2,1)} %add_convert_fusion.1) | copy-start | bytes 2359300
  496.0 39.3 %copy-start.6 = (f32[2048]{0:T(1024)S(1)}, f32[2048]{0:T(1024)}, u32[]{:S(2)}) copy-start(f32[2048]{0:T(1024)} %param.25) | copy-start | bytes 24580
  496.0 39.3 %copy-start.7 = (f32[2048]{0:T(1024)S(1)}, f32[2048]{0:T(1024)}, u32[]{:S(2)}) copy-start(f32[2048]{0:T(1024)} %param.24) | copy-start | bytes 24580
  532.2 3.2 copy-start.3
Sparse Core Ops, SparseCore 0:
  170.1 36.8 reduce-scatter.2
  496.1 35.9 reduce-scatter.4
Sparse Core Ops, SparseCore 1:
  172.7 91.1 all-gather.6
  265.3 26.5 all-gather.4
  293.7 92.9 all-gather.10
  388.9 90.3 all-gather.8
